TPU v7x, 32 devices: a whole 2x2x4 slice. The times are simulated.
32 devices in a mesh: grp: 2 (over y), sp: 4 (over z), tp: 4 (over x, core).
Axes of the slice: x: 2, y: 2, z: 4, core: 2. Of those that a mesh axis runs over, the one named last changes fastest.
Arguments:
- residual: bfloat16 [1024, 2048], P(('grp', 'sp', 'tp')), parts along dimension 0, may hold values from -6 to 6
- receptance: bfloat16 [1024, 2048], P(('grp', 'sp'), 'tp'), parts along dimension 0, may hold values from -6 to 6
- key_in: bfloat16 [1024, 2048], P(('grp', 'sp'), 'tp'), parts along dimension 0, may hold values from -6 to 6
- value_in: bfloat16 [1024, 2048], P(('grp', 'sp'), 'tp'), parts along dimension 0, may hold values from -6 to 6
- log_decay: float32 [1024, 2048], P(('grp', 'sp'), 'tp'), parts along dimension 0, may hold values from -1 to 0, as said below
- rate_pre: bfloat16 [1024, 2048], P(('grp', 'sp'), 'tp'), parts along dimension 0, may hold values from -11 to 3
- out_gate: bfloat16 [1024, 2048], P(('grp', 'sp'), 'tp'), parts along dimension 0, may hold values from -6 to 6
- group_gain: float32 [2048], P('tp'), may hold values from 0.1 to 1.9
- w_out: bfloat16 [2048, 2048], P('tp'), may hold values from -0.125 to 0.125
- norm_gain: float32 [2048], replicated, may hold values from 0.1 to 1.9
- w_gate: bfloat16 [2048, 5632], P('sp', 'tp'), may hold values from -0.125 to 0.125
- w_value: bfloat16 [2048, 5632], P('sp', 'tp'), may hold values from -0.125 to 0.125
- conv_gate: float32 [3, 5632], P(None, 'tp'), may hold values from -3 to 3
- conv_value: float32 [3, 5632], P(None, 'tp'), may hold values from -3 to 3
- w_down: bfloat16 [5632, 2048], P('tp', 'sp'), may hold values from -0.078125 to 0.078125
Outputs:
- layer_out: bfloat16 [1024, 2048], P(('grp', 'sp', 'tp')), parts along dimension 0
There are 2 independent parts, one for each index of `grp`. A program takes and returns all parts, laid end to end along the dimension named above; an argument that names none is the same for every part. Nothing has to cross between parts.
Inputs may be any that keep to these rules, and one draw needn't show every extreme that they name: `log_decay`: every entry is negative.
All inputs are finite; a program needn't handle non-finite values.
Results may differ from a plain program's by a relative error of at most 0.017.
Values may be sent and summed in bfloat16 or wider, within the bound.
A program may use at most 64 MiB of HBM per device.

v0:
```python
import jax
import jax.numpy as jnp
from jax import lax
from jax.sharding import PartitionSpec as P

HEAD = 64


group_eps = 0.00064
norm_eps = 1e-06
highest = lax.Precision.HIGHEST
span_steps = 32


def entering_2(shard, axis, combine, identity):
    count, place = (lax.axis_size(axis), lax.axis_index(axis))
    everything = jax.tree.map(
        lambda part, kind: lax.all_gather(part.astype(kind), axis),
        shard,
        (jnp.bfloat16, jnp.bfloat16),
    )
    start = jax.tree.map(
        lambda part, zero: jnp.broadcast_to(jnp.asarray(zero, part.dtype), part.shape),
        shard,
        identity,
    )

    def lap(k, before):
        reached = k < place
        new = combine(
            before, jax.tree.map(lambda part, own: part[k].astype(own.dtype), everything, shard)
        )
        return jax.tree.map(lambda a, b: jnp.where(reached, a, b), new, before)

    return lax.fori_loop(0, count, lap, start)


def passed_along(shard, axis, by):
    count = lax.axis_size(axis)
    pairs = [(i, i + by) for i in range(count) if 0 <= i + by < count]
    return lax.ppermute(shard, axis, pairs)


def advance(matrix, unit_row, decay_row, pushed):
    removed = jnp.einsum("hij,hj->hi", matrix, -unit_row, precision=highest)
    return matrix * decay_row[:, None, :] + removed[:, :, None] * pushed[:, None, :]


def span_pass(carry, inputs):
    product, partial_state = carry
    recept, decays, keys_all, values, unit_keys, rates = inputs
    local_out = []
    carried = []
    for position in range(span_steps):
        pushed = unit_keys[position] * rates[position]
        product = advance(product, unit_keys[position], decays[position], pushed)
        partial_state = advance(partial_state, unit_keys[position], decays[position], pushed)
        partial_state = (
            partial_state + values[position][:, :, None] * keys_all[position][:, None, :]
        )
        local_out.append(
            jnp.einsum("hvk,hk->hv", partial_state, recept[position], precision=highest)
        )
        carried.append(jnp.einsum("hij,hj->hi", product, recept[position], precision=highest))
    return ((product, partial_state), (jnp.stack(local_out), jnp.stack(carried)))


def combine_spans(earlier, later):
    first_prod, first_state = earlier
    second_prod, second_state = later
    joined_prod = jnp.einsum("hij,hjk->hik", first_prod, second_prod, precision=highest)
    joined_state = (
        jnp.einsum("hij,hjk->hik", first_state, second_prod, precision=highest) + second_state
    )
    return (joined_prod, joined_state)


def group_norm(outputs, group_gain):
    center = jnp.mean(outputs, axis=-1, keepdims=True)
    spread = jnp.mean(jnp.square(outputs - center), axis=-1, keepdims=True)
    scaled = (outputs - center) * lax.rsqrt(spread + group_eps)
    return scaled * group_gain.reshape(-1, HEAD)


def rms_rows(hidden_rows, norm_gain):
    scale = lax.rsqrt(jnp.mean(hidden_rows * hidden_rows, axis=-1, keepdims=True) + norm_eps)
    return (hidden_rows * scale * norm_gain).astype(jnp.bfloat16)


def shards(
    residual,
    receptance,
    key_in,
    value_in,
    log_decay,
    rate_pre,
    out_gate,
    group_gain,
    w_out,
    norm_gain,
    w_gate,
    w_value,
    conv_gate,
    conv_value,
    w_down,
):
    tok_rows, width_loc = receptance.shape
    heads_loc = width_loc // HEAD
    spans = tok_rows // span_steps

    def heads_view(array):
        return array.astype(jnp.float32).reshape(tok_rows, heads_loc, HEAD)

    def span_view(array):
        return array.reshape(spans, span_steps, heads_loc, HEAD)

    keys_all = heads_view(key_in)
    unit_keys = keys_all * lax.rsqrt(
        jnp.sum(keys_all * keys_all, axis=-1, keepdims=True) + norm_eps
    )
    inputs = (
        span_view(heads_view(receptance)),
        span_view(jnp.exp(heads_view(log_decay))),
        span_view(keys_all),
        span_view(heads_view(value_in)),
        span_view(unit_keys),
        span_view(jax.nn.sigmoid(heads_view(rate_pre))),
    )
    identity_prod = jnp.broadcast_to(jnp.eye(HEAD, dtype=jnp.float32), (heads_loc, HEAD, HEAD))
    zero_state = jnp.zeros((heads_loc, HEAD, HEAD), jnp.float32)
    (span_prod, span_state), (local_out, carried) = lax.scan(
        span_pass, (identity_prod, zero_state), inputs
    )
    _, entering = entering_2(
        (span_prod, span_state), "sp", combine_spans, (identity_prod, zero_state)
    )
    local_out = local_out.reshape(tok_rows, heads_loc, HEAD)
    carried = carried.reshape(tok_rows, heads_loc, HEAD)
    mix = local_out + jnp.einsum("hvk,thk->thv", entering, carried, precision=highest)
    normed_mix = group_norm(mix, group_gain).reshape(tok_rows, width_loc)
    mixed = (normed_mix * out_gate.astype(jnp.float32)).astype(jnp.bfloat16)
    picked = mixed
    attended = lax.psum_scatter(
        jnp.dot(picked, w_out, preferred_element_type=jnp.float32).astype(jnp.bfloat16),
        "tp",
        scatter_dimension=0,
        tiled=True,
    ).astype(jnp.float32)
    hidden_own = residual.astype(jnp.float32) + attended
    normed_rows = lax.all_gather(rms_rows(hidden_own, norm_gain), "tp", axis=0, tiled=True)
    gate_up = jnp.dot(
        normed_rows,
        lax.all_gather(w_gate, "sp", axis=0, tiled=True),
        preferred_element_type=jnp.float32,
    )
    value_up = jnp.dot(
        normed_rows,
        lax.all_gather(w_value, "sp", axis=0, tiled=True),
        preferred_element_type=jnp.float32,
    )
    joined = jnp.concatenate([gate_up.astype(jnp.bfloat16), value_up.astype(jnp.bfloat16)], axis=1)
    before = passed_along(joined[-2:], "sp", 1)
    padded = jnp.concatenate([before, joined], axis=0).astype(jnp.float32)
    taps = jnp.concatenate([conv_gate, conv_value], axis=1)
    convolved = taps[0] * padded[:-2] + taps[1] * padded[1:-1] + taps[2] * padded[2:]
    half_width = w_gate.shape[1]
    hidden_ffn = (jax.nn.silu(convolved[:, :half_width]) * convolved[:, half_width:]).astype(
        jnp.bfloat16
    )
    down_full = lax.all_gather(w_down, "sp", axis=1, tiled=True)
    picked = hidden_ffn
    ffn_sum = lax.psum_scatter(
        jnp.dot(picked, down_full, preferred_element_type=jnp.float32).astype(jnp.bfloat16),
        "tp",
        scatter_dimension=0,
        tiled=True,
    ).astype(jnp.float32)
    return (hidden_own + ffn_sum).astype(jnp.bfloat16)


def solution(mesh):
    in_specs = (
        P(("grp", "sp", "tp"), None),
        P(("grp", "sp"), "tp"),
        P(("grp", "sp"), "tp"),
        P(("grp", "sp"), "tp"),
        P(("grp", "sp"), "tp"),
        P(("grp", "sp"), "tp"),
        P(("grp", "sp"), "tp"),
        P("tp"),
        P("tp", None),
        P(),
        P("sp", "tp"),
        P("sp", "tp"),
        P(None, "tp"),
        P(None, "tp"),
        P("tp", "sp"),
    )
    out_specs = P(("grp", "sp", "tp"), None)
    return jax.shard_map(shards, mesh=mesh, in_specs=in_specs, out_specs=out_specs, check_vma=False)
```

profile of v0, /device:TPU:0, one launch (start us, length us, event | category | flops | bytes accessed | tf_op | source)
XLA Modules:
  0.0 1006.3 jit_solution(16631543782656408726)
XLA Ops:
  19.3 585.1 %while.31 = (s32[]{:T(128)}, f32[8,64,64]{2,1,0:T(8,128)S(1)}, f32[8,64,64]{2,1,0:T(8,128)S(1)}, f32[4,32,8,64]{3,2,1,0:T(8,128)}, f32[4,32,8,64]{3,2,1,0:T(8,12...) while((s32[]{:T(128)}, f32[8,64,64]{2,1,0:T(8,128)S(1)}, ...), condition=%wide.region_2.3_spmd.clone, body=%wide.region_1.2_spmd.clone.sunk | while | flops 112885792 | bytes 27522424 | solution.py:131
  42.4 3.0 multiply_add_fusion.413
  48.6 4.1 multiply_add_fusion.414
  55.8 4.8 multiply_add_fusion.415
  63.7 6.0 multiply_add_fusion.416
  98.9 7.0 multiply_add_fusion.417
  123.1 2.2 multiply_add_fusion.406
  127.8 2.8 multiply_add_fusion.407
  133.2 3.3 multiply_add_fusion.408
  159.2 3.8 multiply_add_fusion.409
  187.4 3.0 multiply_add_fusion.413
  193.5 4.1 multiply_add_fusion.414
  200.7 4.8 multiply_add_fusion.415
  208.6 6.0 multiply_add_fusion.416
  243.8 7.0 multiply_add_fusion.417
  272.7 2.8 multiply_add_fusion.407
  278.1 3.3 multiply_add_fusion.408
  304.1 3.8 multiply_add_fusion.409
  332.3 3.0 multiply_add_fusion.413
  338.4 4.1 multiply_add_fusion.414
  345.6 4.8 multiply_add_fusion.415
  353.5 6.0 multiply_add_fusion.416
  388.7 7.0 multiply_add_fusion.417
  417.7 2.8 multiply_add_fusion.407
  423.0 3.3 multiply_add_fusion.408
  449.0 3.8 multiply_add_fusion.409
  477.2 3.0 multiply_add_fusion.413
  483.3 4.1 multiply_add_fusion.414
  490.5 4.8 multiply_add_fusion.415
  498.4 6.0 multiply_add_fusion.416
  533.6 7.0 multiply_add_fusion.417
  557.8 2.2 multiply_add_fusion.406
  562.6 2.8 multiply_add_fusion.407
  567.9 3.3 multiply_add_fusion.408
  593.9 3.8 multiply_add_fusion.409
  604.4 18.0 %all-gather = bf16[32,64,64]{2,1,0:T(8,128)(2,1)} all-gather(bf16[8,64,64]{2,1,0:T(8,128)(2,1)S(1)} %convert_element_type.73), channel_id=2, replica_groups=mesh['grp'=2,'sp'=4,'tp'=4] {'sp'}, dimensions={0}, use_global_device_ids=true | all-gather | bytes 327680 | tf_op jit(solution)/shard_map/all_gather | solution.py:18
  622.4 16.4 %all-gather.1 = bf16[32,64,64]{2,1,0:T(8,128)(2,1)S(1)} all-gather(bf16[8,64,64]{2,1,0:T(8,128)(2,1)S(1)} %convert_element_type.74), channel_id=3, replica_groups=mesh['grp'=2,'sp'=4,'tp'=4] {'sp'}, dimensions={0}, use_global_device_ids=true | all-gather | bytes 327680 | tf_op jit(solution)/shard_map/all_gather | solution.py:18
  638.8 5.7 while.32
  645.8 2.3 fusion.407
  651.7 21.1 %reduce-scatter.3.cloned.1.call-done = bf16[32,2048]{1,0:T(8,128)(2,1)} async-done(((bf16[128,2048]{1,0:T(8,128)(2,1)}), bf16[32,2048]{1,0:T(8,128)(2,1)}) %reduce-scatter.3.cloned.1.call-update) | async-done | bytes 131088 | tf_op jit(solution)/shard_map/reduce_scatter | solution.py:143
  674.8 6.6 all_gather.28
  681.5 78.1 %all-gather.8.cloned.1.call-done = bf16[2048,1408]{1,0:T(8,128)(2,1)} async-done(((bf16[512,1408]{1,0:T(8,128)(2,1)}), bf16[2048,1408]{1,0:T(8,128)(2,1)}) %all-gather.8.cloned.1.call-update) | async-done | bytes 5767184 | tf_op jit(solution)/shard_map/all_gather | solution.py:158
  759.6 3.6 convolution_convert_fusion.2
  763.2 102.6 %all-gather.6.cloned.1.call-done = bf16[2048,1408]{1,0:T(8,128)(2,1)} async-done(((bf16[512,1408]{1,0:T(8,128)(2,1)}), bf16[2048,1408]{1,0:T(8,128)(2,1)}) %all-gather.6.cloned.1.call-update) | async-done | bytes 5767184 | tf_op jit(solution)/shard_map/all_gather | solution.py:153
  865.9 3.6 convolution_convert_fusion.3
  872.8 99.4 %all-gather.10.cloned.1.call-done = bf16[1408,2048]{1,0:T(8,128)(2,1)} async-done(((bf16[1408,512]{1,0:T(8,128)(2,1)}), bf16[1408,2048]{1,0:T(8,128)(2,1)}) %all-gather.10.cloned.1.call-update) | async-done | bytes 5767184 | tf_op jit(solution)/shard_map/all_gather | solution.py:170
  972.2 4.5 convolution_convert_fusion.1
  976.6 20.0 %reduce-scatter.5.cloned.1.call-done = bf16[32,2048]{1,0:T(8,128)(2,1)} async-done(((bf16[128,2048]{1,0:T(8,128)(2,1)}), bf16[32,2048]{1,0:T(8,128)(2,1)}) %reduce-scatter.5.cloned.1.call-update) | async-done | bytes 131088 | tf_op jit(solution)/shard_map/reduce_scatter | solution.py:172
  (1355 shorter events, 459.8 us)
Async XLA Ops:
  7.4 641.1 %copy-start = (bf16[512,2048]{1,0:T(8,128)(2,1)S(1)}, bf16[512,2048]{1,0:T(8,128)(2,1)}, u32[]{:S(2)}) copy-start(bf16[512,2048]{1,0:T(8,128)(2,1)} %param.27) | copy-start | bytes 6291460
  7.4 665.4 %reduce-scatter.3.cloned.1.call-start = ((), (), s32[]{:S(2)}) async-start(), calls=%async_computation.2 | async-start | bytes 655360 | tf_op jit(solution)/shard_map/reduce_scatter | solution.py:143
  61.8 8.4 copy-start.6
  61.8 8.4 copy-start.7
  61.8 8.4 copy-start.33
  61.8 8.4 copy-start.44
  61.8 8.4 copy-start.48
  62.6 8.3 copy-start.32
  62.6 8.3 copy-start.47
  62.6 8.3 copy-start.51
  63.6 8.1 copy-start.46
  97.8 8.6 copy-start.20
  206.7 8.4 copy-start.6
  206.7 8.4 copy-start.7
  206.7 8.4 copy-start.33
  206.7 8.4 copy-start.44
  206.7 8.4 copy-start.48
  207.5 8.3 copy-start.32
  207.5 8.3 copy-start.47
  207.5 8.3 copy-start.51
  208.5 8.1 copy-start.46
  242.7 8.6 copy-start.20
  351.6 8.4 copy-start.6
  351.6 8.4 copy-start.7
  351.6 8.4 copy-start.33
  351.6 8.4 copy-start.44
  351.6 8.4 copy-start.48
  352.4 8.3 copy-start.32
  352.4 8.3 copy-start.47
  352.4 8.3 copy-start.51
  353.4 8.1 copy-start.46
  387.6 8.6 copy-start.20
  496.5 8.4 copy-start.6
  496.5 8.4 copy-start.7
  496.6 8.4 copy-start.33
  496.6 8.4 copy-start.44
  496.6 8.4 copy-start.48
  497.4 8.3 copy-start.32
  497.4 8.3 copy-start.47
  497.4 8.3 copy-start.51
  532.5 8.6 copy-start.20
  649.8 109.8 %all-gather.8.cloned.1.call-start = ((), (), s32[]{:S(2)}) async-start(), calls=%async_computation.4 | async-start | bytes 7208960 | tf_op jit(solution)/shard_map/all_gather | solution.py:158
  650.4 22.4 %copy-start.16 = (bf16[32,2048]{1,0:T(8,128)(2,1)S(1)}, bf16[32,2048]{1,0:T(8,128)(2,1)}, u32[]{:S(2)}) copy-start(bf16[32,2048]{1,0:T(8,128)(2,1)} %param.19) | copy-start | bytes 393220
  650.4 23.4 %copy-start.59 = (f32[2048]{0:T(1024)S(1)}, f32[2048]{0:T(1024)}, u32[]{:S(2)}) copy-start(f32[2048]{0:T(1024)} %param.28) | copy-start | bytes 24580
  650.4 215.4 %all-gather.6.cloned.1.call-start = ((), (), s32[]{:S(2)}) async-start(), calls=%async_computation.3 | async-start | bytes 7208960 | tf_op jit(solution)/shard_map/all_gather | solution.py:153
  651.0 321.1 %all-gather.10.cloned.1.call-start = ((), (), s32[]{:S(2)}) async-start(), calls=%async_computation.5 | async-start | bytes 7208960 | tf_op jit(solution)/shard_map/all_gather | solution.py:170
  651.6 345.1 %reduce-scatter.5.cloned.1.call-start = ((), (), s32[]{:S(2)}) async-start(), calls=%async_computation.6 | async-start | bytes 655360 | tf_op jit(solution)/shard_map/reduce_scatter | solution.py:172
  869.5 2.7 collective-permute-start
  (181 other events, 1105.4 us)
Sparse Core Ops, SparseCore 0:
  649.9 22.7 reduce-scatter.2
  976.8 19.8 reduce-scatter.4
Sparse Core Ops, SparseCore 1:
  651.9 107.7 all-gather.7
  761.0 104.8 all-gather.5
  867.3 104.8 all-gather.9
where the time goes:
time: 1010 us
  matrix products  371 us (37%)
  waiting for transfers between devices  324 us (32%)
  other arithmetic  197 us (20%)
  local copies, waits for them, and re-layouts  44.8 us (4%)
  blocking collectives  41 us (4%)
  between operations  15.6 us (2%)
  loops' own time  11.1 us (1%)
    dot_general x256, matrix products, advance(): removed = jnp.einsum('hij,hj->hi', matrix, -unit_row, precision=highest)  174 us
    add x32, other arithmetic, span_pass(): partial_state + values[position][:, :, None] * keys_all[position][:, None...  116 us
    all_gather x1, waiting for transfers between devices, shards(): lax.all_gather(w_gate, 'sp', axis=0, tiled=True)  103 us
    all_gather x1, waiting for transfers between devices, shards(): down_full = lax.all_gather(w_down, 'sp', axis=1, tiled=True)  99.4 us
    dot_general x128, matrix products, span_pass(): jnp.einsum('hvk,hk->hv', partial_state, recept[position], precision=highest)  94.8 us
    dot_general x128, matrix products, span_pass(): jnp.einsum('hij,hj->hi', product, recept[position], precision=highest)  82 us
    all_gather x1, waiting for transfers between devices, shards(): lax.all_gather(w_value, 'sp', axis=0, tiled=True)  78.1 us
    add x32, other arithmetic, advance(): matrix * decay_row[:, None, :] + removed[:, :, None] * pushed[:, None, :]  64.6 us
  transfers between devices with their start and end apart: 6, of which 6 were waited for; matrix products, arithmetic and copies ran while one was open for 1% of the time, Pallas kernels for 0%

commit v1 on v0

v1 whole, which is shorter than its diff:
```python
import functools

import jax
import jax.numpy as jnp
from jax import lax
from jax.experimental import pallas as pl
from jax.experimental.pallas import tpu as pltpu
from jax.sharding import PartitionSpec as P

HEAD = 64
HALO = 16
group_eps = 0.00064
norm_eps = 1e-06
f32 = jnp.float32
bf16 = jnp.bfloat16
MESH = pl.DeviceIdType.MESH


def dot(a, b, dims=((1,), (0,))):
    return lax.dot_general(
        a, b, (dims, ((), ())), precision=lax.Precision.HIGHEST, preferred_element_type=f32
    )


def fast_dot(a, b):
    return jnp.dot(a, b, preferred_element_type=f32)


def inverse(tri, row, col):
    count = tri.shape[0]
    eye = (row == col).astype(f32)
    small = jnp.where(row // 8 == col // 8, tri, 0.0)
    second = dot(small, small)
    fourth = dot(second, second)
    inv = eye - small
    inv = inv + dot(inv, second)
    inv = inv + dot(inv, fourth)
    size = 16
    while size <= count:
        off = jnp.where(
            (row // size == col // size) & (row // (size // 2) != col // (size // 2)), tri, 0.0
        )
        inv = inv - dot(inv, dot(off, inv))
        size *= 2
    return inv


def body(
    S,
    T,
    recept_ref,
    key_ref,
    value_ref,
    decay_ref,
    rate_ref,
    gate_ref,
    gain_ref,
    resid_ref,
    norm_ref,
    taps_g_ref,
    taps_v_ref,
    wo_hbm,
    wg_hbm,
    wv_hbm,
    wd_hbm,
    out_ref,
    wo,
    wg,
    wv,
    wd,
    q_buf,
    o_buf,
    g_buf,
    u_buf,
    enter_buf,
    leave_buf,
    mixed_buf,
    attn_part,
    attn_recv,
    mid_buf,
    norm_send,
    x_buf,
    up_part,
    up_recv,
    up_acc,
    hid_buf,
    down_part,
    down_recv,
    w_sem,
    chain_sem,
    attn_s,
    attn_r,
    x_s,
    x_r,
    up_s,
    up_r,
    hid_s,
    hid_r,
    down_s,
    down_r,
):
    s, t = lax.axis_index("sp"), lax.axis_index("tp")
    me = s * T + t
    N = S * T
    tok, width = recept_ref.shape
    heads = width // HEAD
    R = resid_ref.shape[0]
    K = x_buf.shape[1]

    loads = [
        pltpu.make_async_copy(a, b, w_sem.at[i])
        for i, (a, b) in enumerate(((wo_hbm, wo), (wg_hbm, wg), (wv_hbm, wv), (wd_hbm, wd)))
    ]
    for load in loads:
        load.start()

    barrier = pltpu.get_barrier_semaphore()

    def greet(d, c):
        peer = lax.rem(me + d, N)
        pl.semaphore_signal(
            barrier,
            inc=1,
            device_id={"sp": peer // T, "tp": lax.rem(peer, T)},
            device_id_type=MESH,
        )
        return c

    lax.fori_loop(1, N, greet, 0)

    row = lax.broadcasted_iota(jnp.int32, (tok, tok), 0)
    col = lax.broadcasted_iota(jnp.int32, (tok, tok), 1)
    lower = (row >= col).astype(f32)
    logs = decay_ref[...]
    total = dot(lower, logs)
    middle = total[tok // 2 - 1 : tok // 2, :]
    last = total[tok - 1 : tok, :]
    earlier = total - logs
    hrow = lax.broadcasted_iota(jnp.int32, (HEAD, HEAD), 0)
    hcol = lax.broadcasted_iota(jnp.int32, (HEAD, HEAD), 1)
    for h in range(heads):
        cols = slice(h * HEAD, (h + 1) * HEAD)
        keys = key_ref[:, cols].astype(f32)
        unit = keys * lax.rsqrt(jnp.sum(keys * keys, axis=-1, keepdims=True) + norm_eps)
        push = unit * jax.nn.sigmoid(rate_ref[:, cols].astype(f32))
        vals = value_ref[:, cols].astype(f32)
        rec = recept_ref[:, cols].astype(f32)
        tot, mid, lst, ear = total[:, cols], middle[:, cols], last[:, cols], earlier[:, cols]
        up = jnp.exp(mid - tot)
        to_end = jnp.exp(lst - tot)
        lefts = jnp.concatenate([unit * jnp.exp(ear - mid), rec * jnp.exp(tot - mid)], axis=0)
        rights = jnp.concatenate([push * up, keys * up], axis=0)
        inner = dot(lefts, rights, ((1,), (1,)))
        a_pb = jnp.where(row > col, inner[:tok, :tok], 0.0)
        a_pk = jnp.where(row > col, inner[:tok, tok:], 0.0)
        a_rb = jnp.where(row >= col, inner[tok:, :tok], 0.0)
        a_rk = jnp.where(row >= col, inner[tok:, tok:], 0.0)
        pk_v = dot(a_pk, vals)
        inv = inverse(a_pb, row, col)
        solved = dot(inv, jnp.concatenate([unit * jnp.exp(ear), pk_v], axis=1))
        read = dot(a_rb, solved)
        q_buf[:, cols] = rec * jnp.exp(tot) - read[:, :HEAD]
        o_buf[:, cols] = dot(a_rk, vals) - read[:, HEAD:]
        back = dot(solved, push * to_end, ((0,), (0,)))
        g_buf[h] = jnp.where(hrow == hcol, jnp.exp(lst), 0.0) - back[:HEAD]
        u_buf[h] = dot(vals, keys * to_end, ((0,), (0,))) - back[HEAD:]

    pl.semaphore_wait(barrier, N - 1)

    chain = pltpu.make_async_remote_copy(
        src_ref=leave_buf,
        dst_ref=enter_buf,
        send_sem=chain_sem.at[0],
        recv_sem=chain_sem.at[1],
        device_id={"sp": jnp.minimum(s + 1, S - 1), "tp": t},
        device_id_type=MESH,
    )

    @pl.when(s == 0)
    def _():
        enter_buf[...] = jnp.zeros_like(enter_buf)

    @pl.when(s > 0)
    def _():
        chain.wait_recv()

    @pl.when(s < S - 1)
    def _():
        for h in range(heads):
            rows = slice((h // 2) * HEAD, (h // 2 + 1) * HEAD)
            lanes = slice((h % 2) * HEAD, (h % 2 + 1) * HEAD)
            state = dot(enter_buf[rows, lanes].astype(f32), g_buf[h]) + u_buf[h]
            leave_buf[rows, lanes] = state.astype(bf16)
        chain.start()

    for h in range(heads):
        cols = slice(h * HEAD, (h + 1) * HEAD)
        rows = slice((h // 2) * HEAD, (h // 2 + 1) * HEAD)
        lanes = slice((h % 2) * HEAD, (h % 2 + 1) * HEAD)
        mix = o_buf[:, cols] + dot(
            q_buf[:, cols], enter_buf[rows, lanes].astype(f32), ((1,), (1,))
        )
        away = mix - jnp.mean(mix, axis=-1, keepdims=True)
        spread = jnp.mean(away * away, axis=-1, keepdims=True)
        normed = away * lax.rsqrt(spread + group_eps) * gain_ref[:, cols]
        mixed_buf[:, cols] = (normed * gate_ref[:, cols].astype(f32)).astype(bf16)

    loads[0].wait()
    attn_part[...] = fast_dot(mixed_buf[...], wo[...]).astype(bf16)
    own_rows = pl.ds(pl.multiple_of(t * R, R), R)
    sends = []
    for d in range(1, T):
        to = lax.rem(t + d, T)
        sends.append(
            pltpu.make_async_remote_copy(
                src_ref=attn_part.at[pl.ds(pl.multiple_of(to * R, R), R)],
                dst_ref=attn_recv.at[d],
                send_sem=attn_s.at[d],
                recv_sem=attn_r.at[d],
                device_id={"sp": s, "tp": to},
                device_id_type=MESH,
            )
        )
        sends[-1].start()
    hidden = resid_ref[...].astype(f32) + attn_part[own_rows, :].astype(f32)
    for d in range(1, T):
        sends[d - 1].wait_recv()
        hidden = hidden + attn_recv[d].astype(f32)
    mid_buf[...] = hidden
    scale = lax.rsqrt(jnp.mean(hidden * hidden, axis=-1, keepdims=True) + norm_eps)
    normed = (hidden * scale * norm_ref[...]).astype(bf16)
    for i in range(S):
        norm_send[i] = normed[:, i * K : (i + 1) * K]

    x_buf[:HALO, :] = jnp.zeros((HALO, K), bf16)
    my_x = pl.ds(pl.multiple_of(HALO + me * R, 16), R)

    def x_copy(peer, slot):
        return pltpu.make_async_remote_copy(
            src_ref=norm_send.at[peer // T],
            dst_ref=x_buf.at[my_x],
            send_sem=x_s.at[slot],
            recv_sem=x_r.at[slot],
            device_id={"sp": peer // T, "tp": lax.rem(peer, T)},
            device_id_type=MESH,
        )

    def x_send(d, c):
        x_copy(lax.rem(me + d, N), d).start()
        return c

    lax.fori_loop(1, N, x_send, 0)
    x_buf[my_x, :] = norm_send[s]

    def x_wait(d, c):
        copy = x_copy(lax.rem(me + d, N), d)
        copy.wait_recv()
        copy.wait_send()
        return c

    lax.fori_loop(1, N, x_wait, 0)

    loads[1].wait()
    loads[2].wait()

    def up_copy(d):
        to = lax.rem(s + d, S)
        return pltpu.make_async_remote_copy(
            src_ref=up_part.at[d],
            dst_ref=up_recv.at[d],
            send_sem=up_s.at[d],
            recv_sem=up_r.at[d],
            device_id={"sp": to, "tp": t},
            device_id_type=MESH,
        )

    def up_rows(to):
        return x_buf[pl.ds(pl.multiple_of(to * tok, 16), tok + HALO), :]

    def up_send(d, c):
        rows = up_rows(lax.rem(s + d, S))
        up_part[d, 0] = fast_dot(rows, wg[...]).astype(bf16)
        up_part[d, 1] = fast_dot(rows, wv[...]).astype(bf16)
        up_copy(d).start()
        return c

    lax.fori_loop(1, S, up_send, 0)
    rows = up_rows(s)
    up_acc[0] = fast_dot(rows, wg[...])
    up_acc[1] = fast_dot(rows, wv[...])

    def up_take(d, c):
        copy = up_copy(d)
        copy.wait_recv()
        up_acc[...] = up_acc[...] + up_recv[d].astype(f32)
        return c

    lax.fori_loop(1, S, up_take, 0)

    def conv(which, taps):
        full = up_acc[which].astype(bf16).astype(f32)
        return (
            taps[0:1, :] * full[HALO - 2 : HALO - 2 + tok]
            + taps[1:2, :] * full[HALO - 1 : HALO - 1 + tok]
            + taps[2:3, :] * full[HALO : HALO + tok]
        )

    gated = conv(0, taps_g_ref)
    my_hid = pl.ds(pl.multiple_of(s * tok, tok), tok)
    hid_buf[my_hid, :] = (gated / (1.0 + jnp.exp(-gated)) * conv(1, taps_v_ref)).astype(bf16)

    def hid_copy(d):
        to = lax.rem(s + d, S)
        return pltpu.make_async_remote_copy(
            src_ref=hid_buf.at[my_hid],
            dst_ref=hid_buf.at[my_hid],
            send_sem=hid_s.at[d],
            recv_sem=hid_r.at[d],
            device_id={"sp": to, "tp": t},
            device_id_type=MESH,
        )

    def hid_send(d, c):
        hid_copy(d).start()
        return c

    lax.fori_loop(1, S, hid_send, 0)
    loads[3].wait()

    def down_copy(peer, slot):
        return pltpu.make_async_remote_copy(
            src_ref=down_part.at[pl.ds(pl.multiple_of(peer * R, R), R)],
            dst_ref=down_recv.at[me],
            send_sem=down_s.at[slot],
            recv_sem=down_r.at[slot],
            device_id={"sp": peer // T, "tp": lax.rem(peer, T)},
            device_id_type=MESH,
        )

    def down_block(frm):
        block = pl.ds(pl.multiple_of(frm * tok, tok), tok)
        down_part[block, :] = fast_dot(hid_buf[block, :], wd[...]).astype(bf16)

    down_block(s)
    for j in range(1, T):
        down_copy(s * T + lax.rem(t + j, T), j).start()

    def down_step(d, c):
        hid_copy(d).wait_recv()
        frm = lax.rem(s + S - d, S)
        down_block(frm)

        def one(j, c2):
            down_copy(frm * T + lax.rem(t + j, T), d * T + j).start()
            return c2

        lax.fori_loop(0, T, one, 0)
        return c

    lax.fori_loop(1, S, down_step, 0)
    down_recv[me] = down_part[pl.ds(pl.multiple_of(me * R, R), R), :]

    def down_wait(e, c):
        frm = lax.rem(s + S - e // T, S)
        copy = down_copy(frm * T + lax.rem(t + lax.rem(e, T), T), e)
        copy.wait_recv()
        copy.wait_send()
        return c

    lax.fori_loop(1, N, down_wait, 0)
    for i in range(S):
        lanes = slice(i * K, (i + 1) * K)
        summed = down_recv[i * T].astype(f32)
        for j in range(1, T):
            summed = summed + down_recv[i * T + j].astype(f32)
        out_ref[:, lanes] = (mid_buf[:, lanes] + summed).astype(bf16)

    for send in sends:
        send.wait_send()

    def finish(d, c):
        up_copy(d).wait_send()
        hid_copy(d).wait_send()
        return c

    lax.fori_loop(1, S, finish, 0)

    @pl.when(s < S - 1)
    def _():
        chain.wait_send()


def shards(S, T, *args):
    (
        residual,
        receptance,
        key_in,
        value_in,
        log_decay,
        rate_pre,
        out_gate,
        group_gain,
        w_out,
        norm_gain,
        w_gate,
        w_value,
        conv_gate,
        conv_value,
        w_down,
    ) = args
    tok, width = receptance.shape
    heads = width // HEAD
    R, D = residual.shape
    K, F = w_gate.shape
    N = S * T
    vmem = pl.BlockSpec(memory_space=pltpu.VMEM)
    hbm = pl.BlockSpec(memory_space=pl.ANY)
    dma = pltpu.SemaphoreType.DMA
    packed = ((heads + 1) // 2 * HEAD, 2 * HEAD)
    return pl.pallas_call(
        functools.partial(body, S, T),
        out_shape=jax.ShapeDtypeStruct((R, D), bf16),
        in_specs=[vmem] * 11 + [hbm] * 4,
        out_specs=vmem,
        scratch_shapes=[
            pltpu.VMEM(w_out.shape, bf16),
            pltpu.VMEM(w_gate.shape, bf16),
            pltpu.VMEM(w_value.shape, bf16),
            pltpu.VMEM(w_down.shape, bf16),
            pltpu.VMEM((tok, width), f32),
            pltpu.VMEM((tok, width), f32),
            pltpu.VMEM((heads, HEAD, HEAD), f32),
            pltpu.VMEM((heads, HEAD, HEAD), f32),
            pltpu.VMEM(packed, bf16),
            pltpu.VMEM(packed, bf16),
            pltpu.VMEM((tok, width), bf16),
            pltpu.VMEM((tok, D), bf16),
            pltpu.VMEM((T, R, D), bf16),
            pltpu.VMEM((R, D), f32),
            pltpu.VMEM((S, R, K), bf16),
            pltpu.VMEM((HALO + N * R, K), bf16),
            pltpu.VMEM((S, 2, tok + HALO, F), bf16),
            pltpu.VMEM((S, 2, tok + HALO, F), bf16),
            pltpu.VMEM((2, tok + HALO, F), f32),
            pltpu.VMEM((S * tok, F), bf16),
            pltpu.VMEM((N * R, K), bf16),
            pltpu.VMEM((N, R, K), bf16),
            dma((4,)),
            dma((2,)),
            dma((T,)),
            dma((T,)),
            dma((N,)),
            dma((N,)),
            dma((S,)),
            dma((S,)),
            dma((S,)),
            dma((S,)),
            dma((N,)),
            dma((N,)),
        ],
        compiler_params=pltpu.CompilerParams(collective_id=0, has_side_effects=True),
    )(
        receptance,
        key_in,
        value_in,
        log_decay,
        rate_pre,
        out_gate,
        group_gain.reshape(1, -1),
        residual,
        norm_gain.reshape(1, -1),
        conv_gate,
        conv_value,
        w_out,
        w_gate,
        w_value,
        w_down,
    )


def solution(mesh):
    in_specs = (
        P(("grp", "sp", "tp"), None),
        P(("grp", "sp"), "tp"),
        P(("grp", "sp"), "tp"),
        P(("grp", "sp"), "tp"),
        P(("grp", "sp"), "tp"),
        P(("grp", "sp"), "tp"),
        P(("grp", "sp"), "tp"),
        P("tp"),
        P("tp", None),
        P(),
        P("sp", "tp"),
        P("sp", "tp"),
        P(None, "tp"),
        P(None, "tp"),
        P("tp", "sp"),
    )
    out_specs = P(("grp", "sp", "tp"), None)
    return jax.shard_map(
        functools.partial(shards, mesh.shape["sp"], mesh.shape["tp"]),
        mesh=mesh,
        in_specs=in_specs,
        out_specs=out_specs,
        check_vma=False,
    )
```

time: 1010 us -> 189 us (0.19)
  matrix products: 371 us -> 0 us
  waiting for transfers between devices: 324 us -> 0 us
  other arithmetic: 197 us -> 0 us
  Pallas kernels: 0 us -> 188 us
  local copies, waits for them, and re-layouts: 44.8 us -> 1.57 us
  blocking collectives: 41 us -> 0 us
  between operations: 15.6 us -> 0.01 us
  loops' own time: 11.1 us -> 0 us
    dot_general x521 -> x0, matrix products: 371 us -> none  [the longest x256 174 us: advance(): removed = jnp.einsum('hij,hj->hi', matrix, -unit_row, precision=highest)]
    all_gather x3 -> x0, waiting for transfers between devices: 280 us -> none  [the longest x1 103 us: shards(): lax.all_gather(w_gate, 'sp', axis=0, tiled=True)]
    pallas_call x0 -> x1, Pallas kernels: none -> 188 us  [shards(): pl.pallas_call(functools.partial(body, S, T), out_shape=jax.ShapeDtypeStr...]
    add x65 -> x0, other arithmetic: 181 us -> none  [the longest x32 116 us: span_pass(): partial_state + values[position][:, :, None] * keys_all[position][:, None...]
    reduce_scatter x2 -> x0, waiting for transfers between devices: 41.1 us -> none  [the longest x1 21.1 us: shards(): lax.psum_scatter(jnp.dot(picked, w_out, preferred_element_type=jnp.float3...]
    all_gather x3 -> x0, blocking collectives: 41 us -> none  [the longest x2 34.4 us: entering_2(): lax.all_gather(part.astype(kind), axis)]
    mul x25 -> x0, local copies, waits for them, and re-layouts: 21 us -> none  [the longest x16 12.3 us: span_pass(): values[position][:, :, None] * keys_all[position][:, None, :]]
    mul x10 -> x0, other arithmetic: 11.4 us -> none  [the longest x8 10.3 us: span_pass(): pushed = unit_keys[position] * rates[position]]
  transfers between devices with their start and end apart: 6 -> 0, of which waited for: 6 -> 0; matrix products, arithmetic and copies ran while one was open for 1% -> 0% of each run, Pallas kernels for 0% -> 0%
where the time goes in v1:
time: 189 us
  Pallas kernels  188 us (99%)
    pallas_call x1, Pallas kernels, shards(): pl.pallas_call(functools.partial(body, S, T), out_shape=jax.ShapeDtypeStr...  188 us

profile of v1, /device:TPU:0, one launch (start us, length us, event | category | flops | bytes accessed | tf_op | source)
XLA Modules:
  0.0 189.3 jit_solution(1720176337814018111)
XLA Ops:
  0.0 187.8 %shard_map.145 = bf16[32,2048]{1,0:T(8,128)(2,1)} custom-call(bf16[128,512]{1,0:T(8,128)(2,1)} %recept_ref.1, bf16[128,512]{1,0:T(8,128)(2,1)} %key_ref.1, bf16[128,512]{1,0:T(8,128)(2,1)} %value_ref.1, f32[128,512]{1,0:T(8,128)} %decay_ref.1, bf16[128,512]{1,0:T(8,128)(2,1)} %rate_ref.1, bf16[128,512]{1,0:T(8,128)(2,1)} %gate_ref.1, f32[1,512]{1,0:T(1,128)} %bitcast.3, ...), custom_call_target="tpu_custom_call" | custom-call | tf_op jit(solution)/shard_map/pallas_call | solution.py:420
  187.8 1.6 copy.17

commit v2 on v1

--- a/solution.py
+++ b/solution.py
@@ -65,8 +65,7 @@
     wd_hbm,
     out_ref,
     wo,
-    wg,
-    wv,
+    wup,
     wd,
     q_buf,
     o_buf,
@@ -90,8 +89,10 @@
     chain_sem,
     attn_s,
     attn_r,
-    x_s,
-    x_r,
+    xz_s,
+    xz_r,
+    xt_s,
+    xt_r,
     up_s,
     up_r,
     hid_s,
@@ -105,14 +106,27 @@
     tok, width = recept_ref.shape
     heads = width // HEAD
     R = resid_ref.shape[0]
-    K = x_buf.shape[1]
-
+    K = wd.shape[1]
+    par = lax.rem(s, 2)
+
+    my_k = pl.ds(pl.multiple_of(par * K, K), K)
     loads = [
-        pltpu.make_async_copy(a, b, w_sem.at[i])
-        for i, (a, b) in enumerate(((wo_hbm, wo), (wg_hbm, wg), (wv_hbm, wv), (wd_hbm, wd)))
+        pltpu.make_async_copy(a, b, w_sem.at[i]) for i, (a, b) in enumerate(((wo_hbm, wo), (wd_hbm, wd)))
     ]
     for load in loads:
         load.start()
+
+    def swap(own, other):
+        keep = pltpu.make_async_copy(own, wup.at[my_k], w_sem.at[2])
+        give = pltpu.make_async_remote_copy(
+            src_ref=other,
+            dst_ref=wup.at[my_k],
+            send_sem=w_sem.at[3],
+            recv_sem=w_sem.at[4],
+            device_id={"sp": s + 1 - 2 * par, "tp": t},
+            device_id_type=MESH,
+        )
+        return keep, give
 
     barrier = pltpu.get_barrier_semaphore()
 
@@ -127,6 +141,17 @@
         return c
 
     lax.fori_loop(1, N, greet, 0)
+    pl.semaphore_wait(barrier, N - 1)
+
+    @pl.when(par == 0)
+    def _():
+        for copy in swap(wg_hbm, wv_hbm):
+            copy.start()
+
+    @pl.when(par == 1)
+    def _():
+        for copy in swap(wv_hbm, wg_hbm):
+            copy.start()
 
     row = lax.broadcasted_iota(jnp.int32, (tok, tok), 0)
     col = lax.broadcasted_iota(jnp.int32, (tok, tok), 1)
@@ -165,8 +190,6 @@
         g_buf[h] = jnp.where(hrow == hcol, jnp.exp(lst), 0.0) - back[:HEAD]
         u_buf[h] = dot(vals, keys * to_end, ((0,), (0,))) - back[HEAD:]
 
-    pl.semaphore_wait(barrier, N - 1)
-
     chain = pltpu.make_async_remote_copy(
         src_ref=leave_buf,
         dst_ref=enter_buf,
@@ -229,39 +252,72 @@
     mid_buf[...] = hidden
     scale = lax.rsqrt(jnp.mean(hidden * hidden, axis=-1, keepdims=True) + norm_eps)
     normed = (hidden * scale * norm_ref[...]).astype(bf16)
-    for i in range(S):
-        norm_send[i] = normed[:, i * K : (i + 1) * K]
-
-    x_buf[:HALO, :] = jnp.zeros((HALO, K), bf16)
-    my_x = pl.ds(pl.multiple_of(HALO + me * R, 16), R)
-
-    def x_copy(peer, slot):
+    for i in range(S // 2):
+        norm_send[i] = normed[:, i * 2 * K : (i + 1) * 2 * K]
+
+    x_buf[:HALO, :] = jnp.zeros((HALO, 2 * K), bf16)
+
+    def x_rows(place, part):
+        return pl.ds(pl.multiple_of(HALO + (place * T + part) * R, 16), R)
+
+    def xz_copy(d):
+        to = lax.rem(s + d, S)
         return pltpu.make_async_remote_copy(
-            src_ref=norm_send.at[peer // T],
-            dst_ref=x_buf.at[my_x],
-            send_sem=x_s.at[slot],
-            recv_sem=x_r.at[slot],
-            device_id={"sp": peer // T, "tp": lax.rem(peer, T)},
-            device_id_type=MESH,
-        )
-
-    def x_send(d, c):
-        x_copy(lax.rem(me + d, N), d).start()
-        return c
-
-    lax.fori_loop(1, N, x_send, 0)
-    x_buf[my_x, :] = norm_send[s]
-
-    def x_wait(d, c):
-        copy = x_copy(lax.rem(me + d, N), d)
-        copy.wait_recv()
-        copy.wait_send()
-        return c
-
-    lax.fori_loop(1, N, x_wait, 0)
-
-    loads[1].wait()
-    loads[2].wait()
+            src_ref=norm_send.at[to // 2],
+            dst_ref=x_buf.at[x_rows(s, t)],
+            send_sem=xz_s.at[d],
+            recv_sem=xz_r.at[d],
+            device_id={"sp": to, "tp": t},
+            device_id_type=MESH,
+        )
+
+    def xt_copy(d, j, src, rows):
+        return pltpu.make_async_remote_copy(
+            src_ref=src,
+            dst_ref=x_buf.at[rows],
+            send_sem=xt_s.at[d * T + j],
+            recv_sem=xt_r.at[d * T + j],
+            device_id={"sp": s, "tp": lax.rem(t + j, T)},
+            device_id_type=MESH,
+        )
+
+    def xz_send(d, c):
+        xz_copy(d).start()
+        return c
+
+    lax.fori_loop(1, S, xz_send, 0)
+    for j in range(1, T):
+        xt_copy(0, j, norm_send.at[s // 2], x_rows(s, t)).start()
+    x_buf[x_rows(s, t), :] = norm_send[s // 2]
+
+    def x_pass(d, c):
+        xz_copy(d).wait_recv()
+        rows = x_rows(lax.rem(s + S - d, S), t)
+        for j in range(1, T):
+            xt_copy(d, j, x_buf.at[rows], rows).start()
+        return c
+
+    lax.fori_loop(1, S, x_pass, 0)
+
+    def xt_wait(d, c):
+        rows = x_rows(lax.rem(s + S - d, S), t)
+        for j in range(1, T):
+            copy = xt_copy(d, j, x_buf.at[rows], rows)
+            copy.wait_recv()
+            copy.wait_send()
+        return c
+
+    lax.fori_loop(0, S, xt_wait, 0)
+
+    @pl.when(par == 0)
+    def _():
+        for copy in swap(wg_hbm, wv_hbm):
+            copy.wait()
+
+    @pl.when(par == 1)
+    def _():
+        for copy in swap(wv_hbm, wg_hbm):
+            copy.wait()
 
     def up_copy(d):
         to = lax.rem(s + d, S)
@@ -278,21 +334,18 @@
         return x_buf[pl.ds(pl.multiple_of(to * tok, 16), tok + HALO), :]
 
     def up_send(d, c):
-        rows = up_rows(lax.rem(s + d, S))
-        up_part[d, 0] = fast_dot(rows, wg[...]).astype(bf16)
-        up_part[d, 1] = fast_dot(rows, wv[...]).astype(bf16)
+        up_part[d] = fast_dot(up_rows(lax.rem(s + d, S)), wup[...]).astype(bf16)
         up_copy(d).start()
         return c
 
     lax.fori_loop(1, S, up_send, 0)
-    rows = up_rows(s)
-    up_acc[0] = fast_dot(rows, wg[...])
-    up_acc[1] = fast_dot(rows, wv[...])
+    up_acc[par] = fast_dot(up_rows(s), wup[...])
+    up_acc[1 - par] = jnp.zeros(up_acc.shape[1:], f32)
 
     def up_take(d, c):
-        copy = up_copy(d)
-        copy.wait_recv()
-        up_acc[...] = up_acc[...] + up_recv[d].astype(f32)
+        up_copy(d).wait_recv()
+        which = lax.rem(s + S - d, 2)
+        up_acc[which] = up_acc[which] + up_recv[d].astype(f32)
         return c
 
     lax.fori_loop(1, S, up_take, 0)
@@ -325,7 +378,7 @@
         return c
 
     lax.fori_loop(1, S, hid_send, 0)
-    loads[3].wait()
+    loads[1].wait()
 
     def down_copy(peer, slot):
         return pltpu.make_async_remote_copy(
@@ -379,6 +432,7 @@
         send.wait_send()
 
     def finish(d, c):
+        xz_copy(d).wait_send()
         up_copy(d).wait_send()
         hid_copy(d).wait_send()
         return c
@@ -424,8 +478,7 @@
         out_specs=vmem,
         scratch_shapes=[
             pltpu.VMEM(w_out.shape, bf16),
-            pltpu.VMEM(w_gate.shape, bf16),
-            pltpu.VMEM(w_value.shape, bf16),
+            pltpu.VMEM((2 * K, F), bf16),
             pltpu.VMEM(w_down.shape, bf16),
             pltpu.VMEM((tok, width), f32),
             pltpu.VMEM((tok, width), f32),
@@ -437,18 +490,20 @@
             pltpu.VMEM((tok, D), bf16),
             pltpu.VMEM((T, R, D), bf16),
             pltpu.VMEM((R, D), f32),
-            pltpu.VMEM((S, R, K), bf16),
-            pltpu.VMEM((HALO + N * R, K), bf16),
-            pltpu.VMEM((S, 2, tok + HALO, F), bf16),
-            pltpu.VMEM((S, 2, tok + HALO, F), bf16),
+            pltpu.VMEM((S // 2, R, 2 * K), bf16),
+            pltpu.VMEM((HALO + N * R, 2 * K), bf16),
+            pltpu.VMEM((S, tok + HALO, F), bf16),
+            pltpu.VMEM((S, tok + HALO, F), bf16),
             pltpu.VMEM((2, tok + HALO, F), f32),
             pltpu.VMEM((S * tok, F), bf16),
             pltpu.VMEM((N * R, K), bf16),
             pltpu.VMEM((N, R, K), bf16),
-            dma((4,)),
+            dma((5,)),
             dma((2,)),
             dma((T,)),
             dma((T,)),
+            dma((S,)),
+            dma((S,)),
             dma((N,)),
             dma((N,)),
             dma((S,)),

time: 189 us -> 157 us (0.83)
  Pallas kernels: 188 us -> 155 us
    pallas_call x1, Pallas kernels: 188 us -> 155 us  [shards(): pl.pallas_call(functools.partial(body, S, T), out_shape=jax.ShapeDtypeStr...]
where the time goes in v2:
time: 157 us
  Pallas kernels  155 us (99%)
  local copies, waits for them, and re-layouts  1.57 us (1%)
    pallas_call x1, Pallas kernels, shards(): pl.pallas_call(functools.partial(body, S, T), out_shape=jax.ShapeDtypeStr...  155 us

profile of v2, /device:TPU:0, one launch (start us, length us, event | category | flops | bytes accessed | tf_op | source)
XLA Modules:
  0.0 156.7 jit_solution(8955571878739510472)
XLA Ops:
  0.0 155.1 %shard_map.145 = bf16[32,2048]{1,0:T(8,128)(2,1)} custom-call(bf16[128,512]{1,0:T(8,128)(2,1)} %recept_ref.1, bf16[128,512]{1,0:T(8,128)(2,1)} %key_ref.1, bf16[128,512]{1,0:T(8,128)(2,1)} %value_ref.1, f32[128,512]{1,0:T(8,128)} %decay_ref.1, bf16[128,512]{1,0:T(8,128)(2,1)} %rate_ref.1, bf16[128,512]{1,0:T(8,128)(2,1)} %gate_ref.1, f32[1,512]{1,0:T(1,128)} %bitcast.3, ...), custom_call_target="tpu_custom_call" | custom-call | tf_op jit(solution)/shard_map/pallas_call | solution.py:474
  155.1 1.6 %copy.17 = bf16[32,2048]{1,0:T(8,128)(2,1)} copy(bf16[32,2048]{1,0:T(8,128)(2,1)} %shard_map.145) | data formatting | bytes 262144
